TPU v7x, 32 devices: a whole 2x2x4 slice. The times are simulated.
32 devices in a mesh: grp: 2 (over y), fs: 4 (over z), tp: 4 (over x, core).
Axes of the slice: x: 2, y: 2, z: 4, core: 2. Of those that a mesh axis runs over, the one named last changes fastest.
Arguments:
- tokens: bfloat16 [4096, 2048], P(('grp', 'fs')), parts along dimension 0, may hold values from -6 to 6
- pre_gain: float32 [2048], replicated, may hold values from 0.1 to 1.9
- gate_weight: float32 [2048, 5632], P('fs', 'tp'), may hold values from -0.125 to 0.125
- gate_scale: float32 [5632], P('tp'), may hold values from 0.5 to 2
- up_weight: float32 [2048, 5632], P('fs', 'tp'), may hold values from -0.125 to 0.125
- up_scale: float32 [5632], P('tp'), may hold values from 0.5 to 2
- down_weight: float32 [5632, 2048], P('tp', 'fs'), may hold values from -0.078125 to 0.078125
- down_scale: float32 [2048], replicated, may hold values from 0.3 to 3
- post_gain: float32 [2048], replicated, may hold values from 0.1 to 1.9
Outputs:
- mixed: bfloat16 [4096, 2048], P(('grp', 'fs')), parts along dimension 0
There are 2 independent parts, one for each index of `grp`. A program takes and returns all parts, laid end to end along the dimension named above; an argument that names none is the same for every part. Nothing has to cross between parts.
All inputs are finite; a program needn't handle non-finite values.
Results may differ from a plain program's by a relative error of at most 0.018.
Values may be sent and summed in bfloat16 or wider, within the bound.
A program may use at most 64 MiB of HBM per device.

v0:
```python
import jax
import jax.numpy as jnp
from jax import lax
from jax.sharding import PartitionSpec as P

EPS = 1e-06


def finish(summed, down_scale, post_gain):
    branch = summed * down_scale
    return (
        branch * lax.rsqrt(jnp.mean(branch * branch, axis=-1, keepdims=True) + EPS) * post_gain
    ).astype(jnp.bfloat16)


def gather_shards(block):
    groups, shards = (lax.axis_size("grp"), lax.axis_size("fs"))
    rows, columns = block.shape
    pieces = block.reshape(groups, rows // groups, columns)
    mine = lax.dynamic_index_in_dim(pieces, lax.axis_index("grp"), 0, keepdims=False)
    whole = lax.all_gather(mine, ("fs", "grp"), axis=0, tiled=True)
    return whole.reshape(shards, rows, columns)


def gather_shared(block):
    whole = gather_shards(block)
    return whole.reshape(-1, block.shape[1])


def body(
    tokens,
    pre_gain,
    gate_weight,
    gate_scale,
    up_weight,
    up_scale,
    down_weight,
    down_scale,
    post_gain,
):
    rows = tokens.astype(jnp.float32)
    normed = (
        rows * lax.rsqrt(jnp.mean(rows * rows, axis=-1, keepdims=True) + EPS) * pre_gain
    ).astype(jnp.bfloat16)
    gate_low = gate_weight.astype(jnp.bfloat16)
    up_low = up_weight.astype(jnp.bfloat16)
    down_low = down_weight.astype(jnp.bfloat16)
    gate_full, up_full = (gather_shared(gate_low), gather_shared(up_low))
    gate = jnp.dot(normed, gate_full, preferred_element_type=jnp.float32) * gate_scale
    up = jnp.dot(normed, up_full, preferred_element_type=jnp.float32) * up_scale
    hidden = (jax.nn.silu(gate) * up).astype(jnp.bfloat16)
    shards = gather_shards(down_low)
    partial_value = jnp.concatenate(
        [
            jnp.dot(hidden, shards[k], preferred_element_type=jnp.float32)
            for k in range(shards.shape[0])
        ],
        axis=1,
    )
    summed = lax.psum(partial_value.astype(jnp.bfloat16), "tp").astype(jnp.float32)
    return finish(summed, down_scale, post_gain)


def solution(mesh):
    in_specs = (
        P(("grp", "fs"), None),
        P(),
        P("fs", "tp"),
        P("tp"),
        P("fs", "tp"),
        P("tp"),
        P("tp", "fs"),
        P(),
        P(),
    )
    out_specs = P(("grp", "fs"), None)
    return jax.shard_map(body, mesh=mesh, in_specs=in_specs, out_specs=out_specs, check_vma=False)
```

profile of v0, /device:TPU:0, one launch (start us, length us, event | category | flops | bytes accessed | tf_op | source)
XLA Modules:
  0.0 360.9 jit_solution(10505173811535307966)
XLA Ops:
  6.5 2.0 convert_element_type.27
  8.5 0.9 constant_dynamic-slice_fusion.2
  9.5 0.0 all-gather.9.cloned.1.call-start
  9.5 2.1 convert_element_type.28
  11.6 0.9 constant_dynamic-slice_fusion.1
  12.6 0.0 all-gather.11.cloned.1.call-start
  12.6 0.2 convert_element_type.30
  12.9 0.9 constant_dynamic-slice_fusion
  13.9 0.8 copy-done.2
  14.7 0.5 fusion.4
  15.2 89.5 %all-gather.7.cloned.1.call-done = bf16[1,2048,1408]{2,1,0:T(8,128)(2,1)} async-done(((bf16[1,256,1408]{2,1,0:T(8,128)(2,1)}), bf16[1,2048,1408]{2,1,0:T(8,128)(2,1)}) %all-gather.7.cloned.1.call-update) | async-done | bytes 5767184 | tf_op jit(solution)/shard_map/all_gather | solution.py:21
  104.6 7.6 %fusion.7 = f32[512,1408]{1,0:T(8,128)} fusion(bf16[1,2048,1408]{2,1,0:T(8,128)(2,1)} %all-gather.7.cloned.1.call-done, f32[1408]{0:T(1024)S(1)} %copy-done.6, bf16[512,2048]{1,0:T(8,128)(2,1)S(1)} %copy-done.2, f32[2048]{0:T(1024)S(1)} %copy-done.7, f32[512]{0:T(512)S(1)} %add_rsqrt_fusion.1), kind=kOutput, calls=%fused_computation.12 | convolution fusion | flops 2957705216 | bytes 10763776 | tf_op jit(solution)/shard_map/dot_general | solution.py:49
  112.3 85.1 %all-gather.9.cloned.1.call-done = bf16[1,2048,1408]{2,1,0:T(8,128)(2,1)} async-done(((bf16[1,256,1408]{2,1,0:T(8,128)(2,1)}), bf16[1,2048,1408]{2,1,0:T(8,128)(2,1)}) %all-gather.9.cloned.1.call-update) | async-done | bytes 5767184 | tf_op jit(solution)/shard_map/all_gather | solution.py:21
  197.3 7.8 %fusion.16 = bf16[512,1408]{1,0:T(8,128)(2,1)} fusion(bf16[1,2048,1408]{2,1,0:T(8,128)(2,1)} %all-gather.9.cloned.1.call-done, f32[512,1408]{1,0:T(8,128)} %fusion.7, f32[1408]{0:T(1024)S(1)} %copy-done.8, bf16[512,2048]{1,0:T(8,128)(2,1)S(1)} %copy-done.2, f32[2048]{0:T(1024)S(1)} %copy-done.7, f32[512]{0:T(512)S(1)} %add_rsqrt_fusion.1), kind=kOutput, calls=%fused_computation.15 | convolution fusion | flops 2962030592 | bytes 12205568 | tf_op jit(solution)/shard_map/dot_general | solution.py:50
  205.2 84.9 %all-gather.11.cloned.1.call-done = bf16[1,5632,512]{2,1,0:T(8,128)(2,1)} async-done(((bf16[1,704,512]{2,1,0:T(8,128)(2,1)}), bf16[1,5632,512]{2,1,0:T(8,128)(2,1)}) %all-gather.11.cloned.1.call-update) | async-done | bytes 5767184 | tf_op jit(solution)/shard_map/all_gather | solution.py:21
  290.1 3.0 fusion.25
  293.0 2.4 fusion.24
  295.5 1.0 fusion.23
  296.5 1.0 fusion.26
  297.5 1.5 pad_maximum_fusion
  299.0 49.7 %all-reduce.2.cloned.1.call-done = bf16[512,2048]{0,1:T(8,128)(2,1)} async-done(((bf16[512,2048]{0,1:T(8,128)(2,1)}), bf16[512,2048]{0,1:T(8,128)(2,1)}) %all-reduce.2.cloned.1.call-update) | async-done | bytes 2097168 | tf_op jit(solution)/shard_map/psum | solution.py:60
  348.7 2.4 multiply_reduce_fusion
  351.1 0.9 multiply_convert_fusion
  352.0 2.4 copy.10
  (27 shorter events, 0.2 us)
Async XLA Ops:
  6.5 98.1 %all-gather.7.cloned.1.call-start = ((), (), s32[]{:S(2)}) async-start(), calls=%async_computation.1 | async-start | bytes 6488064 | tf_op jit(solution)/shard_map/all_gather | solution.py:21
  9.5 3.2 copy-start.1
  9.5 187.9 %all-gather.9.cloned.1.call-start = ((), (), s32[]{:S(2)}) async-start(), calls=%async_computation.2 | async-start | bytes 6488064 | tf_op jit(solution)/shard_map/all_gather | solution.py:21
  12.6 277.5 %all-gather.11.cloned.1.call-start = ((), (), s32[]{:S(2)}) async-start(), calls=%async_computation.3 | async-start | bytes 6488064 | tf_op jit(solution)/shard_map/all_gather | solution.py:21
  12.8 1.9 copy-start.2
  12.8 91.8 %copy-start.6 = (f32[1408]{0:T(1024)S(1)}, f32[1408]{0:T(1024)}, u32[]{:S(2)}) copy-start(f32[1408]{0:T(1024)} %param.12) | copy-start | bytes 16900
  12.9 91.8 %copy-start.7 = (f32[2048]{0:T(1024)S(1)}, f32[2048]{0:T(1024)}, u32[]{:S(2)}) copy-start(f32[2048]{0:T(1024)} %param.10) | copy-start | bytes 24580
  13.8 334.9 %all-reduce.2.cloned.1.call-start = ((), (), s32[]{:S(2)}) async-start(), calls=%async_computation | async-start | bytes 4194304 | tf_op jit(solution)/shard_map/psum | solution.py:60
  15.2 182.2 %copy-start.8 = (f32[1408]{0:T(1024)S(1)}, f32[1408]{0:T(1024)}, u32[]{:S(2)}) copy-start(f32[1408]{0:T(1024)} %param.14) | copy-start | bytes 16900
  205.2 87.9 %copy-start.9 = (bf16[512,1408]{1,0:T(8,128)(2,1)S(1)}, bf16[512,1408]{1,0:T(8,128)(2,1)}, u32[]{:S(2)}) copy-start(bf16[512,1408]{1,0:T(8,128)(2,1)} %fusion.16) | copy-start | bytes 4325380
  290.1 5.4 %copy-start.5 = (bf16[1,5632,512]{2,1,0:T(8,128)(2,1)S(1)}, bf16[1,5632,512]{2,1,0:T(8,128)(2,1)}, u32[]{:S(2)}) copy-start(bf16[1,5632,512]{2,1,0:T(8,128)(2,1)} %all-gather.11.cloned.1.call-done) | copy-start | bytes 17301508
  297.5 51.2 %copy-start.3 = (f32[2048]{0:T(1024)S(1)}, f32[2048]{0:T(1024)}, u32[]{:S(2)}) copy-start(f32[2048]{0:T(1024)} %param.16) | copy-start | bytes 24580
  299.0 52.1 %copy-start.4 = (f32[2048]{0:T(1024)S(1)}, f32[2048]{0:T(1024)}, u32[]{:S(2)}) copy-start(f32[2048]{0:T(1024)} %param.17) | copy-start | bytes 24580
  348.7 2.4 copy-start
Sparse Core Ops, SparseCore 0:
  9.6 95.0 all-gather.6
  106.8 90.4 all-gather.8
  199.5 90.4 all-gather.10
  299.1 49.5 all-reduce.1
where the time goes:
time: 361 us
  waiting for transfers between devices  309 us (86%)
  matrix products  22.9 us (6%)
  between operations  13.3 us (4%)
  other arithmetic  9.44 us (3%)
  local copies, waits for them, and re-layouts  6.02 us (2%)
    all_gather x3, waiting for transfers between devices, gather_shards(): whole = lax.all_gather(mine, ('fs', 'grp'), axis=0, tiled=True)  259 us
    psum x1, waiting for transfers between devices, body(): lax.psum(partial_value.astype(jnp.bfloat16), 'tp').astype(jnp.float32)  49.7 us
    dot_general x1, matrix products, body(): up = jnp.dot(normed, up_full, preferred_element_type=jnp.float32) * up_scale  7.8 us
    dot_general x1, matrix products, body(): jnp.dot(normed, gate_full, preferred_element_type=jnp.float32) * gate_scale  7.64 us
    dot_general x4, matrix products, body(): jnp.dot(hidden, shards[k], preferred_element_type=jnp.float32)  7.42 us
  transfers between devices with their start and end apart: 4, of which 4 were waited for; matrix products, arithmetic and copies ran while one was open for 6% of the time, Pallas kernels for 0%

commit v1 on v0

--- a/solution.py
+++ b/solution.py
@@ -57,7 +57,9 @@
         ],
         axis=1,
     )
-    summed = lax.psum(partial_value.astype(jnp.bfloat16), "tp").astype(jnp.float32)
+    summed = jnp.sum(lax.all_gather(partial_value.astype(jnp.bfloat16), "tp"), axis=0).astype(
+        jnp.float32
+    )
     return finish(summed, down_scale, post_gain)
 
 

time: 361 us -> 380 us (1.053)
  waiting for transfers between devices: 309 us -> 316 us
  local copies, waits for them, and re-layouts: 6.02 us -> 12.8 us
  other arithmetic: 9.44 us -> 14.6 us
    all_gather x0 -> x1, waiting for transfers between devices: none -> 56.6 us  [body(): lax.all_gather(partial_value.astype(jnp.bfloat16), 'tp')]
    psum x1 -> x0, waiting for transfers between devices: 49.7 us -> none  [body(): lax.psum(partial_value.astype(jnp.bfloat16), 'tp').astype(jnp.float32)]
    reduce_sum x0 -> x1, other arithmetic: none -> 7.2 us  [body(): jnp.sum(lax.all_gather(partial_value.astype(jnp.bfloat16), 'tp'), axis=0)]
  transfers between devices with their start and end apart: 4 -> 4, of which waited for: 4 -> 4; matrix products, arithmetic and copies ran while one was open for 6% -> 5% of each run, Pallas kernels for 0% -> 0%
where the time goes in v1:
time: 380 us
  waiting for transfers between devices  316 us (83%)
  matrix products  22.9 us (6%)
  other arithmetic  14.6 us (4%)
  between operations  13.3 us (4%)
  local copies, waits for them, and re-layouts  12.8 us (3%)
    all_gather x3, waiting for transfers between devices, gather_shards(): whole = lax.all_gather(mine, ('fs', 'grp'), axis=0, tiled=True)  259 us
    all_gather x1, waiting for transfers between devices, body(): lax.all_gather(partial_value.astype(jnp.bfloat16), 'tp')  56.6 us
    dot_general x1, matrix products, body(): up = jnp.dot(normed, up_full, preferred_element_type=jnp.float32) * up_scale  7.8 us
    dot_general x1, matrix products, body(): jnp.dot(normed, gate_full, preferred_element_type=jnp.float32) * gate_scale  7.65 us
  transfers between devices with their start and end apart: 4, of which 4 were waited for; matrix products, arithmetic and copies ran while one was open for 5% of the time, Pallas kernels for 0%

profile of v1, /device:TPU:0, one launch (start us, length us, event | category | flops | bytes accessed | tf_op | source)
XLA Modules:
  0.0 379.7 jit_solution(3486667154467788923)
XLA Ops:
  6.5 2.0 convert_element_type.36
  8.5 0.9 constant_dynamic-slice_fusion.2
  9.5 2.1 convert_element_type.37
  11.6 0.9 constant_dynamic-slice_fusion.1
  12.6 0.2 convert_element_type.39
  12.9 0.9 constant_dynamic-slice_fusion
  13.9 0.8 copy-done.1
  14.7 0.5 fusion.4
  15.2 89.5 %all-gather.10.cloned.1.call-done = bf16[1,2048,1408]{2,1,0:T(8,128)(2,1)} async-done(((bf16[1,256,1408]{2,1,0:T(8,128)(2,1)}), bf16[1,2048,1408]{2,1,0:T(8,128)(2,1)}) %all-gather.10.cloned.1.call-update) | async-done | bytes 5767184 | tf_op jit(solution)/shard_map/all_gather | solution.py:21
  104.6 7.6 %fusion.7 = f32[512,1408]{1,0:T(8,128)} fusion(bf16[1,2048,1408]{2,1,0:T(8,128)(2,1)} %all-gather.10.cloned.1.call-done, f32[1408]{0:T(1024)S(1)} %copy-done.5, bf16[512,2048]{1,0:T(8,128)(2,1)S(1)} %copy-done.1, f32[2048]{0:T(1024)S(1)} %copy-done.6, f32[512]{0:T(512)S(1)} %add_rsqrt_fusion.1), kind=kOutput, calls=%fused_computation.12 | convolution fusion | flops 2957705216 | bytes 10763776 | tf_op jit(solution)/shard_map/dot_general | solution.py:49
  112.3 85.1 %all-gather.12.cloned.1.call-done = bf16[1,2048,1408]{2,1,0:T(8,128)(2,1)} async-done(((bf16[1,256,1408]{2,1,0:T(8,128)(2,1)}), bf16[1,2048,1408]{2,1,0:T(8,128)(2,1)}) %all-gather.12.cloned.1.call-update) | async-done | bytes 5767184 | tf_op jit(solution)/shard_map/all_gather | solution.py:21
  197.3 7.8 %fusion.16 = bf16[512,1408]{1,0:T(8,128)(2,1)} fusion(bf16[1,2048,1408]{2,1,0:T(8,128)(2,1)} %all-gather.12.cloned.1.call-done, f32[512,1408]{1,0:T(8,128)} %fusion.7, f32[1408]{0:T(1024)S(1)} %copy-done.7, bf16[512,2048]{1,0:T(8,128)(2,1)S(1)} %copy-done.1, f32[2048]{0:T(1024)S(1)} %copy-done.6, f32[512]{0:T(512)S(1)} %add_rsqrt_fusion.1), kind=kOutput, calls=%fused_computation.15 | convolution fusion | flops 2962030592 | bytes 12205568 | tf_op jit(solution)/shard_map/dot_general | solution.py:50
  205.2 84.9 %all-gather.14.cloned.1.call-done = bf16[1,5632,512]{2,1,0:T(8,128)(2,1)} async-done(((bf16[1,704,512]{2,1,0:T(8,128)(2,1)}), bf16[1,5632,512]{2,1,0:T(8,128)(2,1)}) %all-gather.14.cloned.1.call-update) | async-done | bytes 5767184 | tf_op jit(solution)/shard_map/all_gather | solution.py:21
  290.1 3.0 fusion.28
  293.0 2.4 fusion.29
  295.4 1.0 fusion.30
  296.5 1.0 fusion.27
  297.7 2.4 copy.10
  300.1 56.6 %all-gather.8.cloned.1.call-done = bf16[4,512,2048]{2,1,0:T(8,128)(2,1)} async-done(((bf16[1,512,2048]{2,1,0:T(8,128)(2,1)}), bf16[4,512,2048]{2,1,0:T(8,128)(2,1)}) %all-gather.8.cloned.1.call-update) | async-done | bytes 8388624 | tf_op jit(solution)/shard_map/all_gather | solution.py:60
  356.7 7.2 %reduce_sum.31 = bf16[512,2048]{1,0:T(8,128)(2,1)} reduce(bf16[4,512,2048]{2,1,0:T(8,128)(2,1)} %all-gather.8.cloned.1.call-done, bf16[]{:T(256)} %constant.30.clone.1), dimensions={0}, to_apply=%region_1.2 | reduce | flops 3145728 | bytes 10485762 | tf_op jit(solution)/shard_map/reduce_sum | solution.py:60
  363.9 2.9 copy.13
  366.8 0.6 multiply_reduce_fusion
  367.4 1.9 multiply_convert_fusion
  369.3 3.9 %copy.12 = bf16[512,2048]{1,0:T(8,128)(2,1)} copy(bf16[512,2048]{0,1:T(8,128)(2,1)} %multiply_convert_fusion) | data formatting | bytes 4194304 | tf_op jit(solution)/shard_map/convert_element_type | solution.py:13
  (28 shorter events, 0.4 us)
Async XLA Ops:
  6.5 98.1 %all-gather.10.cloned.1.call-start = ((), (), s32[]{:S(2)}) async-start(), calls=%async_computation.1 | async-start | bytes 6488064 | tf_op jit(solution)/shard_map/all_gather | solution.py:21
  9.5 3.2 copy-start
  9.5 187.9 %all-gather.12.cloned.1.call-start = ((), (), s32[]{:S(2)}) async-start(), calls=%async_computation.2 | async-start | bytes 6488064 | tf_op jit(solution)/shard_map/all_gather | solution.py:21
  12.6 277.5 %all-gather.14.cloned.1.call-start = ((), (), s32[]{:S(2)}) async-start(), calls=%async_computation.3 | async-start | bytes 6488064 | tf_op jit(solution)/shard_map/all_gather | solution.py:21
  12.8 1.9 copy-start.1
  12.8 91.8 %copy-start.5 = (f32[1408]{0:T(1024)S(1)}, f32[1408]{0:T(1024)}, u32[]{:S(2)}) copy-start(f32[1408]{0:T(1024)} %param.12) | copy-start | bytes 16900
  12.9 91.8 %copy-start.6 = (f32[2048]{0:T(1024)S(1)}, f32[2048]{0:T(1024)}, u32[]{:S(2)}) copy-start(f32[2048]{0:T(1024)} %param.10) | copy-start | bytes 24580
  13.8 342.9 %all-gather.8.cloned.1.call-start = ((), (), s32[]{:S(2)}) async-start(), calls=%async_computation | async-start | bytes 10485760 | tf_op jit(solution)/shard_map/all_gather | solution.py:60
  15.2 182.2 %copy-start.7 = (f32[1408]{0:T(1024)S(1)}, f32[1408]{0:T(1024)}, u32[]{:S(2)}) copy-start(f32[1408]{0:T(1024)} %param.14) | copy-start | bytes 16900
  205.2 87.9 %copy-start.8 = (bf16[512,1408]{1,0:T(8,128)(2,1)S(1)}, bf16[512,1408]{1,0:T(8,128)(2,1)}, u32[]{:S(2)}) copy-start(bf16[512,1408]{1,0:T(8,128)(2,1)} %fusion.16) | copy-start | bytes 4325380
  290.1 5.4 %copy-start.4 = (bf16[1,5632,512]{2,1,0:T(8,128)(2,1)S(1)}, bf16[1,5632,512]{2,1,0:T(8,128)(2,1)}, u32[]{:S(2)}) copy-start(bf16[1,5632,512]{2,1,0:T(8,128)(2,1)} %all-gather.14.cloned.1.call-done) | copy-start | bytes 17301508
  363.9 2.9 copy-start.2
  363.9 3.5 copy-start.3
Sparse Core Ops, SparseCore 0:
  9.6 95.0 all-gather.9
  106.8 90.4 all-gather.11
  199.5 90.4 all-gather.13
  300.2 56.4 all-gather.7
